TPU v7x, 1024 devices: a whole 4x4x32 slice. The times are simulated.
1024 devices in a mesh: ep: 64 (over z, core), tp: 16 (over y, x).
Axes of the slice: x: 4, y: 4, z: 32, core: 2. Of those that a mesh axis runs over, the one named last changes fastest.
Arguments:
- tokens: bfloat16 [32768, 2048], P('ep', 'tp'), may hold values from -3000 to 3000
- norm_gain: float32 [2048], replicated, may hold values from 0.1 to 1.9
- gate_weight: bfloat16 [64, 2048, 512], P('ep'), may hold values from -0.125 to 0.125
- up_weight: bfloat16 [64, 2048, 512], P('ep'), may hold values from -0.125 to 0.125
- down_weight: bfloat16 [64, 512, 2048], P('ep'), may hold values from -0.25 to 0.25
- expert_ids: int32 [32768, 2], P('ep'), may hold values from 0 to 63, as said below
- route_weight: float32 [32768, 2], P('ep'), may hold values from 0.2 to 1
Outputs:
- mixed: bfloat16 [32768, 2048], P('ep', 'tp')
Inputs may be any that keep to these rules, and one draw needn't show every extreme that they name: `expert_ids`: A token's two experts differ and lie in one group of 8 consecutive experts. In each aligned block of 32 rows no expert is named more than 2 times, and in every block all experts of one group, the same group for all blocks, are named exactly 2 times.
All inputs are finite; a program needn't handle non-finite values.
Results may differ from a plain program's by a relative error of at most 0.0071.
Values may be sent and summed in bfloat16 or wider, within the bound.
A program may use at most 32 MiB of HBM per device.

v0:
```python
from functools import partial

import jax
import jax.numpy as jnp
from jax import lax
from jax.sharding import PartitionSpec as P


def slot_numbers(block_ids, experts):
    flat_ids = block_ids.reshape(-1)
    hit_table = (flat_ids[:, None] == jnp.arange(experts, dtype=jnp.int32)[None, :]).astype(
        jnp.int32
    )
    earlier = jnp.cumsum(hit_table, axis=0) - hit_table
    return (flat_ids, jnp.sum(earlier * hit_table, axis=1))


def placement_matrix(flat_ids, slot_index, experts, capacity):
    target = (flat_ids * capacity + slot_index).reshape(-1, 2)
    slot_rows = jnp.arange(experts * capacity, dtype=jnp.int32)[:, None]
    first_hit = (target[:, 0][None, :] == slot_rows).astype(jnp.bfloat16)
    second_hit = (target[:, 1][None, :] == slot_rows).astype(jnp.bfloat16)
    return first_hit + second_hit


def expert_apply(row_data, gate_weight, up_weight, down_weight):
    shape_in = row_data.shape
    flat_rows = row_data.reshape(-1, shape_in[-1])
    gate_part = jnp.dot(flat_rows, gate_weight[0], preferred_element_type=jnp.float32)
    up_part = jnp.dot(flat_rows, up_weight[0], preferred_element_type=jnp.float32)
    hidden = (jax.nn.silu(gate_part) * up_part).astype(jnp.bfloat16)
    produced = jnp.dot(hidden, down_weight[0], preferred_element_type=jnp.float32).astype(
        jnp.bfloat16
    )
    return produced.reshape(shape_in[:-1] + (produced.shape[-1],))


def local(tokens, norm_gain, gate_weight, up_weight, down_weight, expert_ids, route_weight):
    tp_count = lax.axis_size("tp")
    experts = lax.axis_size("ep") * gate_weight.shape[0]
    model_width = gate_weight.shape[1]
    group_rows = tokens.shape[0]
    block_rows = group_rows // tp_count
    capacity = 4 * block_rows // experts
    tp_index = lax.axis_index("tp")
    apply_experts = partial(
        expert_apply, gate_weight=gate_weight, up_weight=up_weight, down_weight=down_weight
    )
    full_rows = lax.all_to_all(tokens, "tp", split_axis=0, concat_axis=1, tiled=True)
    block_ids = lax.dynamic_slice_in_dim(expert_ids, tp_index * block_rows, block_rows, 0)
    block_weight = lax.dynamic_slice_in_dim(route_weight, tp_index * block_rows, block_rows, 0)
    widened = full_rows.astype(jnp.float32)
    mean_square = jnp.mean(widened * widened, axis=-1, keepdims=True)
    normed = (widened * lax.rsqrt(mean_square + 1e-06) * norm_gain).astype(jnp.bfloat16)
    flat_ids, slot_index = slot_numbers(block_ids, experts)
    placing = placement_matrix(flat_ids, slot_index, experts, capacity)
    outgoing = jnp.dot(placing, normed, preferred_element_type=jnp.float32).astype(jnp.bfloat16)
    outgoing = outgoing.reshape(experts, capacity, model_width)
    produced = apply_experts(
        lax.all_to_all(outgoing, "ep", split_axis=0, concat_axis=0, tiled=True)
    )
    returned = lax.all_to_all(produced, "ep", split_axis=0, concat_axis=0, tiled=True)
    picked = jnp.take(returned.reshape(-1, model_width), flat_ids * capacity + slot_index, axis=0)
    weighted = picked.astype(jnp.float32) * block_weight.reshape(-1)[:, None]
    mixed_rows = weighted.reshape(block_rows, 2, model_width).sum(axis=1).astype(jnp.bfloat16)
    return lax.all_to_all(mixed_rows, "tp", split_axis=1, concat_axis=0, tiled=True)


def solution(mesh):
    in_specs = (
        P("ep", "tp"),
        P(),
        P("ep", None, None),
        P("ep", None, None),
        P("ep", None, None),
        P("ep", None),
        P("ep", None),
    )
    out_specs = P("ep", "tp")
    return jax.shard_map(local, mesh=mesh, in_specs=in_specs, out_specs=out_specs, check_vma=False)
```

profile of v0, /device:TPU:1, one launch (start us, length us, event | category | flops | bytes accessed | tf_op | source)
XLA Modules:
  0.0 201.1 jit_solution(1341979886868479442)
XLA Ops:
  0.0 0.0 copy-start
  0.0 7.7 %all-to-all-start = ((bf16[16,32,128]{2,1,0:T(8,128)(2,1)}), bf16[16,32,128]{2,1,0:T(8,128)(2,1)S(1)}, u32[]{:S(2)}, u32[]{:S(2)}) async-start(bf16[16,32,128]{2,1,0:T(8,128)(2,1)} %bitcast.51), calls=%async_computation | async-start | bytes 262144 | tf_op jit(solution)/shard_map/all_to_all | solution.py:49
  7.7 0.8 broadcast_multiply_fusion
  8.5 0.1 copy.21
  8.6 0.1 reshape.87
  8.7 0.1 fusion.32
  8.7 0.1 reduce_window_sum.11
  8.8 0.2 select_reduce_fusion
  9.0 0.1 reduce_sum.32
  9.1 0.1 copy.22
  9.3 5.3 %all-to-all-done = bf16[16,32,128]{2,1,0:T(8,128)(2,1)S(1)} async-done(((bf16[16,32,128]{2,1,0:T(8,128)(2,1)}), bf16[16,32,128]{2,1,0:T(8,128)(2,1)S(1)}, u32[]{:S(2)}, u32[]{:S(2)}) %all-to-all-start) | async-done | bytes 131104 | tf_op jit(solution)/shard_map/all_to_all | solution.py:49
  14.6 0.1 fusion.13
  14.7 1.0 convolution_convert_fusion.1
  15.8 0.3 reshape.88
  16.1 94.8 %all_to_all.39 = bf16[64,2,2048]{2,1,0:T(2,128)(2,1)} all-to-all(bf16[64,2,2048]{2,1,0:T(2,128)(2,1)S(1)} %reshape.88), channel_id=1, replica_groups=mesh['ep'=64,'tp'=16] {'ep'}, dimensions={0} | all-to-all | bytes 1048576 | tf_op jit(solution)/shard_map/all_to_all | solution.py:60
  110.9 1.2 reshape.89
  112.2 2.0 %fusion.3 = f32[128,512]{1,0:T(8,128)S(1)} fusion(bf16[128,2048]{1,0:T(8,128)(2,1)S(1)} %reshape.89, bf16[1,2048,512]{2,1,0:T(8,128)(2,1)} %param.9), kind=kOutput, calls=%fused_computation.6 | convolution fusion | flops 268435456 | bytes 2883584 | tf_op jit(solution)/shard_map/dot_general | solution.py:29
  114.2 0.0 copy-done
  114.2 2.4 %convolution_convert_fusion = bf16[128,2048]{1,0:T(8,128)(2,1)S(1)} fusion(bf16[1,512,2048]{2,1,0:T(8,128)(2,1)S(1)} %copy-done, bf16[128,2048]{1,0:T(8,128)(2,1)S(1)} %reshape.89, bf16[1,2048,512]{2,1,0:T(8,128)(2,1)} %param.10, f32[128,512]{1,0:T(8,128)S(1)} %fusion.3), kind=kOutput, calls=%fused_computation.1 | convolution fusion | flops 537526272 | bytes 5505024 | tf_op jit(solution)/shard_map/dot_general | solution.py:32
  116.6 1.1 reshape.90
  117.8 6.3 %all-to-all-start.2 = ((bf16[64,2,2048]{2,1,0:T(2,128)(2,1)}), bf16[64,2,2048]{2,1,0:T(2,128)(2,1)S(1)}, u32[]{:S(2)}, u32[]{:S(2)}) async-start(bf16[64,2,2048]{2,1,0:T(2,128)(2,1)} %reshape.90), calls=%async_computation.2 | async-start | bytes 1048576 | tf_op jit(solution)/shard_map/all_to_all | solution.py:62
  124.1 0.1 copy.25
  124.2 0.1 mul.72
  124.3 0.1 copy.23
  124.4 0.8 constant_dynamic-slice_fusion
  125.2 0.1 copy.26
  125.3 62.7 %all-to-all-done.2 = bf16[64,2,2048]{2,1,0:T(2,128)(2,1)S(1)} async-done(((bf16[64,2,2048]{2,1,0:T(2,128)(2,1)}), bf16[64,2,2048]{2,1,0:T(2,128)(2,1)S(1)}, u32[]{:S(2)}, u32[]{:S(2)}) %all-to-all-start.2) | async-done | bytes 524320 | tf_op jit(solution)/shard_map/all_to_all | solution.py:62
  188.0 0.2 reshape.91
  188.2 0.7 gather_fusion
  188.9 0.2 gather.7
  189.1 1.6 multiply_reduce_fusion
  190.8 9.6 %all_to_all.40 = bf16[32,16,128]{2,0,1:T(8,128)(2,1)S(1)} all-to-all(bf16[32,16,128]{2,0,1:T(8,128)(2,1)S(1)} %copy_bitcast_fusion), channel_id=1, replica_groups=mesh['ep'=64,'tp'=16] {'tp'}, dimensions={1} | all-to-all | bytes 262144 | tf_op jit(solution)/shard_map/all_to_all | solution.py:66
  200.4 0.7 copy.34
  (6 shorter events, 0.1 us)
Async XLA Ops:
  0.0 114.2 %copy-start = (bf16[1,512,2048]{2,1,0:T(8,128)(2,1)S(1)}, bf16[1,512,2048]{2,1,0:T(8,128)(2,1)}, u32[]{:S(2)}) copy-start(bf16[1,512,2048]{2,1,0:T(8,128)(2,1)} %param.11) | copy-start | bytes 6291460
  0.0 14.6 %all-to-all-start = ((bf16[16,32,128]{2,1,0:T(8,128)(2,1)}), bf16[16,32,128]{2,1,0:T(8,128)(2,1)S(1)}, u32[]{:S(2)}, u32[]{:S(2)}) async-start(bf16[16,32,128]{2,1,0:T(8,128)(2,1)} %bitcast.51), calls=%async_computation | async-start | bytes 262144 | tf_op jit(solution)/shard_map/all_to_all | solution.py:49
  117.8 70.2 %all-to-all-start.2 = ((bf16[64,2,2048]{2,1,0:T(2,128)(2,1)}), bf16[64,2,2048]{2,1,0:T(2,128)(2,1)S(1)}, u32[]{:S(2)}, u32[]{:S(2)}) async-start(bf16[64,2,2048]{2,1,0:T(2,128)(2,1)} %reshape.90), calls=%async_computation.2 | async-start | bytes 1048576 | tf_op jit(solution)/shard_map/all_to_all | solution.py:62
where the time goes:
time: 203 us; the launch traced here: 201 us
  blocking collectives  104 us (51%)
  waiting for transfers between devices  68 us (33%)
  starting transfers between devices  14 us (7%)
  local copies, waits for them, and re-layouts  6.04 us (3%)
  matrix products  5.5 us (3%)
  other arithmetic  2.91 us (1%)
    all_to_all x1, blocking collectives, local(): lax.all_to_all(outgoing, 'ep', split_axis=0, concat_axis=0, tiled=True)  94.8 us
    all_to_all x1, waiting for transfers between devices, local(): lax.all_to_all(produced, 'ep', split_axis=0, concat_axis=0, tiled=True)  62.7 us
    all_to_all x1, blocking collectives, local(): lax.all_to_all(mixed_rows, 'tp', split_axis=1, concat_axis=0, tiled=True)  9.64 us
    all_to_all x1, starting transfers between devices, local(): lax.all_to_all(tokens, 'tp', split_axis=0, concat_axis=1, tiled=True)  7.7 us
    all_to_all x1, starting transfers between devices, local(): lax.all_to_all(produced, 'ep', split_axis=0, concat_axis=0, tiled=True)  6.33 us
    all_to_all x1, waiting for transfers between devices, local(): lax.all_to_all(tokens, 'tp', split_axis=0, concat_axis=1, tiled=True)  5.3 us
  transfers between devices with their start and end apart: 2, of which 2 were waited for; matrix products, arithmetic and copies ran while one was open for 1% of the time, Pallas kernels for 0%

commit v1 on v0

v1 whole, which is shorter than its diff:
```python
from functools import partial

import jax
import jax.numpy as jnp
from jax import lax
from jax.experimental import pallas as pl
from jax.experimental.pallas import tpu as pltpu
from jax.sharding import PartitionSpec as P

MESH = pl.DeviceIdType.MESH
F32 = jnp.float32
BF16 = jnp.bfloat16
CHIPS = 4
EPG = 8
SLOTS = 8


def dot(a, b, contract=((1,), (0,))):
    return lax.dot_general(a, b, (contract, ((), ())), preferred_element_type=F32)


def to_row(col):
    n = col.shape[0]
    eye = lax.broadcasted_iota(jnp.int32, (n, n), 0) == lax.broadcasted_iota(jnp.int32, (n, n), 1)
    return jnp.sum(jnp.where(eye, col, jnp.zeros_like(col)), axis=0, keepdims=True)


def body(
    ep_count, tp_count,
    tokens, gain, gate_hbm, up_hbm, down_hbm, ids_hbm, wts_hbm,
    out,
    xin, ids, wts, gate, up, down, xn, sb, rbuf, sbuf, xe, yo, pbuf, obuf, ret, mx,
    w_sem, in_sem, tp_send, tp_recv, s1, r1, s2, r2, s3, r3, s4, r4, fin_send, fin_recv,
):
    e = lax.axis_index("ep")
    t = lax.axis_index("tp")
    groups = ep_count // EPG
    half = groups // 2
    nbatch = half
    c = lax.rem(e, 2)
    z = e // 2
    p = lax.rem(z, CHIPS)
    g = z // CHIPS
    rows = xn.shape[0]
    width = gate.shape[0]
    is_relay = lax.rem(p, 3) == 0
    my_e = 2 * p + c

    weight_copies = [
        pltpu.make_async_copy(gate_hbm.at[0], gate, w_sem.at[0]),
        pltpu.make_async_copy(up_hbm.at[0], up, w_sem.at[1]),
        pltpu.make_async_copy(down_hbm.at[0], down, w_sem.at[2]),
    ]
    small_copies = [
        pltpu.make_async_copy(ids_hbm.at[pl.ds(t * rows, rows)], ids, in_sem.at[0]),
        pltpu.make_async_copy(wts_hbm.at[pl.ds(t * rows, rows)], wts, in_sem.at[1]),
        pltpu.make_async_copy(tokens.at[pl.ds(t * rows, rows)], xin.at[t], in_sem.at[2]),
    ]
    for cp in small_copies:
        cp.start()
    barrier = pltpu.get_barrier_semaphore()

    @pl.loop(1, ep_count)
    def _(k):
        pl.semaphore_signal(barrier, inc=1, device_id={"ep": lax.rem(e + k, ep_count)}, device_id_type=MESH)

    if tp_count > 1:
        @pl.loop(1, tp_count)
        def _(k):
            pl.semaphore_signal(barrier, inc=1, device_id={"tp": lax.rem(t + k, tp_count)}, device_id_type=MESH)

    for cp in weight_copies:
        cp.start()

    for cp in small_copies[:2]:
        cp.wait()
    idv = ids[...]
    wv = wts[...]
    lane2 = lax.broadcasted_iota(jnp.int32, idv.shape, 1)
    id_col = [jnp.sum(jnp.where(lane2 == k, idv, 0), axis=1, keepdims=True) for k in range(2)]
    w_col = [jnp.sum(jnp.where(lane2 == k, wv, 0.0), axis=1, keepdims=True) for k in range(2)]
    id_row = [to_row(v) for v in id_col]
    before = lax.broadcasted_iota(jnp.int32, (rows, rows), 1) < lax.broadcasted_iota(jnp.int32, (rows, rows), 0)
    g_col = id_col[0] // EPG
    same = before & ((id_row[0] // EPG) == g_col)
    rank = jnp.sum(jnp.where(same, 1, 0), axis=1, keepdims=True)
    rel = lax.rem(g_col - g + groups, groups)
    target = rel * SLOTS + rank
    q_col = []
    for k in range(2):
        hit = jnp.where(id_row[0] == id_col[k], 1, 0) + jnp.where(id_row[1] == id_col[k], 1, 0)
        q_col.append(jnp.sum(jnp.where(before, hit, 0), axis=1, keepdims=True))
    lane = lax.broadcasted_iota(jnp.int32, (rows, 128), 1)
    lane_lo = lax.rem(lane, 64)
    w_tok = jnp.zeros((rows, 128), F32)
    for k in range(2):
        high = w_col[k].astype(BF16).astype(F32)
        part = jnp.where(lane < 64, high, w_col[k] - high)
        on = (lane_lo // 8 == lax.rem(id_col[k], EPG)) & (lax.rem(lane, 2) == q_col[k])
        w_tok = w_tok + jnp.where(on, part, 0.0)
    xn[:, width:] = w_tok.astype(BF16)
    place = jnp.where(
        lax.broadcasted_iota(jnp.int32, (groups * SLOTS, rows), 0) == to_row(target), 1.0, 0.0
    ).astype(BF16)
    unplace = jnp.where(
        lax.broadcasted_iota(jnp.int32, (rows, groups * SLOTS), 1) == target, 1.0, 0.0
    ).astype(BF16)

    pl.semaphore_wait(barrier, ep_count - 1 + (tp_count - 1))

    if tp_count > 1:
        @pl.loop(1, tp_count)
        def _(k):
            peer = lax.rem(t + k, tp_count)
            pltpu.make_async_remote_copy(
                src_ref=tokens.at[pl.ds(peer * rows, rows)], dst_ref=xin.at[t],
                send_sem=tp_send, recv_sem=tp_recv, device_id={"tp": peer}, device_id_type=MESH,
            ).start()

        pltpu.make_async_copy(xin.at[pl.ds(0, tp_count - 1)], xin.at[pl.ds(0, tp_count - 1)], tp_recv).wait()
    small_copies[2].wait()
    piece = xin.shape[2]
    total = jnp.zeros((rows, piece), F32)
    for i in range(tp_count):
        v = xin[i].astype(F32)
        total = total + v * v
    scale = lax.rsqrt(jnp.sum(total, axis=1, keepdims=True) / width + 1e-06)
    for i in range(tp_count):
        cols = slice(i * piece, (i + 1) * piece)
        xn[:, cols] = (xin[i].astype(F32) * scale * gain[:, cols]).astype(BF16)
    placed = dot(place, xn[...])
    for r in range(groups):
        sb[r] = placed[r * SLOTS:(r + 1) * SLOTS].astype(BF16)

    def ep_of(zz):
        return {"ep": zz * 2 + c}

    def send1(r, dest_z, k, b):
        return pltpu.make_async_remote_copy(
            src_ref=sb.at[r], dst_ref=rbuf.at[k, b], send_sem=s1, recv_sem=r1.at[k],
            device_id=ep_of(dest_z), device_id_type=MESH,
        )

    send1(half, lax.rem(g + half, groups) * CHIPS + 3 * (1 - p // 2), nbatch - 1, lax.rem(p, 2)).start()
    for d in range(half - 1, 0, -1):
        send1(d, lax.rem(g + d, groups) * CHIPS, d - 1, p).start()
        send1(groups - d, lax.rem(g + groups - d, groups) * CHIPS + 3, d - 1, p).start()
    own_slot = 2 + lax.rem(p, 2)

    @pl.when(is_relay)
    def _():
        pltpu.make_async_copy(sb.at[0], rbuf.at[nbatch - 1, own_slot], r1.at[nbatch - 1]).start()

    @pl.when(jnp.logical_not(is_relay))
    def _():
        send1(0, g * CHIPS + 3 * (p // 2), nbatch - 1, own_slot).start()

    relay_id = (p // 3) * 2 + c
    row_of = lax.broadcasted_iota(jnp.int32, (32, 64), 0) // SLOTS
    lane_of = lax.rem(lax.broadcasted_iota(jnp.int32, (32, 64), 1) // 2, 4)
    diagonal = row_of == lane_of

    def select(k):
        pltpu.make_async_copy(rbuf.at[k], rbuf.at[k], r1.at[k]).wait()
        got = rbuf[k].reshape(4 * SLOTS, width + 128)
        wide = got[:, width:width + 64].astype(F32)
        sel = jnp.where(diagonal & (wide != 0.0), 1.0, 0.0).astype(BF16)
        chosen = dot(sel, got[:, :width], ((0,), (0,)))
        for ee in range(EPG):
            sbuf[k, ee] = chosen[ee * 8:(ee + 1) * 8].astype(BF16)
        for d in range(1, EPG):
            ee = lax.rem(my_e + d, EPG)
            pltpu.make_async_remote_copy(
                src_ref=sbuf.at[k, ee], dst_ref=xe.at[k, relay_id], send_sem=s2, recv_sem=r2.at[k],
                device_id={"ep": g * EPG + ee}, device_id_type=MESH,
            ).start()
        pltpu.make_async_copy(sbuf.at[k, my_e], xe.at[k, relay_id], r2.at[k]).start()

    def expert(k):
        pltpu.make_async_copy(xe.at[k], xe.at[k], r2.at[k]).wait()
        x = xe[k].reshape(32, width)
        a = dot(x, gate[...])
        b = dot(x, up[...])
        h = (a / (1.0 + jnp.exp(-a)) * b).astype(BF16)
        y = dot(h, down[...])
        for i in range(4):
            yo[k, i] = y[i * 8:(i + 1) * 8].astype(BF16)
        for i in range(4):
            dest = 6 * (i // 2) + i % 2

            @pl.when(my_e == dest)
            def _():
                pltpu.make_async_copy(yo.at[k, i], pbuf.at[k, my_e], r3.at[k]).start()

            @pl.when(my_e != dest)
            def _():
                pltpu.make_async_remote_copy(
                    src_ref=yo.at[k, i], dst_ref=pbuf.at[k, my_e], send_sem=s3, recv_sem=r3.at[k],
                    device_id={"ep": g * EPG + dest}, device_id_type=MESH,
                ).start()

    def combine(k):
        pltpu.make_async_copy(pbuf.at[k], pbuf.at[k], r3.at[k]).wait()
        parts = pbuf[k].reshape(64, width)
        wide = rbuf[k].reshape(4 * SLOTS, width + 128)[:, width:].astype(F32)
        high = jnp.where(diagonal, wide[:, :64], 0.0).astype(BF16)
        low = jnp.where(diagonal, wide[:, 64:], 0.0).astype(BF16)
        y = dot(high, parts) + dot(low, parts)
        for b in range(4):
            obuf[k, b] = y[b * 8:(b + 1) * 8].astype(BF16)
        sign = 1 - 2 * (p // 3)
        for b in range(4):
            if k < nbatch - 1:
                d = k + 1
                src_z = lax.rem(g + groups - sign * d, groups) * CHIPS + b
                r = lax.rem(groups + sign * d, groups)
            elif b < 2:
                src_z = lax.rem(g + half, groups) * CHIPS + 2 * (1 - p // 3) + b
                r = half
            else:
                src_z = g * CHIPS + 2 * (p // 3) + b - 2
                r = 0
            send = pltpu.make_async_remote_copy(
                src_ref=obuf.at[k, b], dst_ref=ret.at[r], send_sem=s4, recv_sem=r4,
                device_id=ep_of(src_z), device_id_type=MESH,
            )
            if k == nbatch - 1 and b >= 2:
                mine = src_z == z

                @pl.when(mine)
                def _():
                    pltpu.make_async_copy(obuf.at[k, b], ret.at[0], r4).start()

                @pl.when(jnp.logical_not(mine))
                def _():
                    send.start()
            else:
                send.start()

    for cp in weight_copies:
        cp.wait()
    order = [nbatch - 1] + list(range(nbatch - 2, -1, -1))
    for step in range(nbatch + 2):
        if step < nbatch:
            @pl.when(is_relay)
            def _():
                select(order[step])
        if 1 <= step <= nbatch:
            expert(order[step - 1])
        if step >= 2:
            @pl.when(is_relay)
            def _():
                combine(order[step - 2])

    pltpu.make_async_copy(ret, ret, r4).wait()
    mixed = dot(unplace, ret[...].reshape(groups * SLOTS, width))
    for i in range(tp_count):
        mx[i] = mixed[:, i * piece:(i + 1) * piece].astype(BF16)
    mine = pltpu.make_async_copy(mx.at[t], out.at[pl.ds(t * rows, rows)], in_sem.at[2])
    mine.start()
    if tp_count > 1:
        @pl.loop(1, tp_count)
        def _(k):
            peer = lax.rem(t + k, tp_count)
            pltpu.make_async_remote_copy(
                src_ref=mx.at[peer], dst_ref=out.at[pl.ds(t * rows, rows)],
                send_sem=fin_send, recv_sem=fin_recv, device_id={"tp": peer}, device_id_type=MESH,
            ).start()

        others = mx.at[pl.ds(0, tp_count - 1)]
        pltpu.make_async_copy(others, others, fin_recv).wait()
        pltpu.make_async_copy(others, others, fin_send).wait()
        others = xin.at[pl.ds(0, tp_count - 1)]
        pltpu.make_async_copy(others, others, tp_send).wait()
    mine.wait()

    @pl.when(is_relay)
    def _():
        n = groups - 1
        pltpu.make_async_copy(sb.at[pl.ds(0, n)], sb.at[pl.ds(0, n)], s1).wait()
        every = sbuf.at[:, pl.ds(0, EPG - 1)]
        pltpu.make_async_copy(every, every, s2).wait()
        every = yo.at[:, pl.ds(0, 3)]
        pltpu.make_async_copy(every, every, s3).wait()
        rest = nbatch * 4 - 1
        flat = obuf.reshape(nbatch * 4, SLOTS, width).at[pl.ds(0, rest)]
        pltpu.make_async_copy(flat, flat, s4).wait()

    @pl.when(jnp.logical_not(is_relay))
    def _():
        pltpu.make_async_copy(sb, sb, s1).wait()
        pltpu.make_async_copy(yo, yo, s3).wait()


def local(tokens, norm_gain, gate_weight, up_weight, down_weight, expert_ids, route_weight, ep_count, tp_count):
    tok, piece = tokens.shape
    rows = tok // tp_count
    _, width, ff = gate_weight.shape
    groups = ep_count // EPG
    nb = groups // 2
    wide = width + 128
    any_spec = pl.BlockSpec(memory_space=pl.ANY)
    vmem_spec = pl.BlockSpec(memory_space=pltpu.VMEM)
    dma = pltpu.SemaphoreType.DMA
    return pl.pallas_call(
        partial(body, ep_count, tp_count),
        out_shape=jax.ShapeDtypeStruct(tokens.shape, BF16),
        in_specs=[any_spec, vmem_spec] + [any_spec] * 5,
        out_specs=any_spec,
        scratch_shapes=[
            pltpu.VMEM((tp_count, rows, piece), BF16),
            pltpu.VMEM((rows, 2), jnp.int32),
            pltpu.VMEM((rows, 2), F32),
            pltpu.VMEM((width, ff), BF16),
            pltpu.VMEM((width, ff), BF16),
            pltpu.VMEM((ff, width), BF16),
            pltpu.VMEM((rows, wide), BF16),
            pltpu.VMEM((groups, SLOTS, wide), BF16),
            pltpu.VMEM((nb, 4, SLOTS, wide), BF16),
            pltpu.VMEM((nb, EPG, 8, width), BF16),
            pltpu.VMEM((nb, 4, 8, width), BF16),
            pltpu.VMEM((nb, 4, 8, width), BF16),
            pltpu.VMEM((nb, EPG, 8, width), BF16),
            pltpu.VMEM((nb, 4, SLOTS, width), BF16),
            pltpu.VMEM((groups, SLOTS, width), BF16),
            pltpu.VMEM((tp_count, rows, piece), BF16),
            dma((3,)), dma((3,)), dma, dma,
            dma, dma((nb,)), dma, dma((nb,)), dma, dma((nb,)), dma, dma, dma, dma,
        ],
        compiler_params=pltpu.CompilerParams(
            collective_id=0, has_side_effects=True, vmem_limit_bytes=50 * 1024 * 1024
        ),
        name="moe",
    )(tokens, norm_gain.reshape(1, width), gate_weight, up_weight, down_weight, expert_ids, route_weight)


def solution(mesh):
    in_specs = (
        P("ep", "tp"),
        P(),
        P("ep", None, None),
        P("ep", None, None),
        P("ep", None, None),
        P("ep", None),
        P("ep", None),
    )
    fn = partial(local, ep_count=mesh.shape["ep"], tp_count=mesh.shape["tp"])
    return jax.shard_map(fn, mesh=mesh, in_specs=in_specs, out_specs=P("ep", "tp"), check_vma=False)
```

time: 203 us -> 121 us (0.60); the launches traced: 201 us -> 121 us
  Pallas kernels: 0 us -> 116 us
  blocking collectives: 104 us -> 0 us
  waiting for transfers between devices: 68 us -> 0 us
  starting transfers between devices: 14 us -> 0 us
  matrix products: 5.5 us -> 0 us
  other arithmetic: 2.91 us -> 0 us
    pallas_call x0 -> x1, Pallas kernels: none -> 116 us  [local(): pl.pallas_call(partial(body, ep_count, tp_count), out_shape=jax.ShapeDtyp...]
    all_to_all x2 -> x0, blocking collectives: 104 us -> none  [the longest x1 94.8 us: local(): lax.all_to_all(outgoing, 'ep', split_axis=0, concat_axis=0, tiled=True)]
    all_to_all x2 -> x0, waiting for transfers between devices: 68 us -> none  [the longest x1 62.7 us: local(): lax.all_to_all(produced, 'ep', split_axis=0, concat_axis=0, tiled=True)]
    all_to_all x2 -> x0, starting transfers between devices: 14 us -> none  [the longest x1 7.7 us: local(): lax.all_to_all(tokens, 'tp', split_axis=0, concat_axis=1, tiled=True)]
    dot_general x3 -> x0, matrix products: 5.5 us -> none  [the longest x1 2.42 us: expert_apply(): jnp.dot(hidden, down_weight[0], preferred_element_type=jnp.float32)]
    unnamed x3 -> x9, local copies, waits for them, and re-layouts: 0.66 us -> 5.5 us
    reshape x5 -> x0, local copies, waits for them, and re-layouts: 3.01 us -> none  [the longest x1 1.24 us: expert_apply(): flat_rows = row_data.reshape(-1, shape_in[-1])]
  transfers between devices with their start and end apart: 2 -> 0, of which waited for: 2 -> 0; matrix products, arithmetic and copies ran while one was open for 1% -> 0% of each run, Pallas kernels for 0% -> 0%
where the time goes in v1:
time: 121 us
  Pallas kernels  116 us (96%)
  local copies, waits for them, and re-layouts  5.5 us (5%)
    pallas_call x1, Pallas kernels, local(): pl.pallas_call(partial(body, ep_count, tp_count), out_shape=jax.ShapeDtyp...  116 us
    unnamed x9, local copies, waits for them, and re-layouts  5.5 us

profile of v1, /device:TPU:1, one launch (start us, length us, event | category | flops | bytes accessed | tf_op | source)
XLA Modules:
  0.0 121.2 jit_solution(12135563083767511848)
XLA Ops:
  0.0 0.8 copy.8.ids_hbm
  0.8 0.8 copy.9.wts_hbm
  1.7 0.0 copy-start
  1.7 1.6 %copy-done = bf16[1,2048,512]{2,1,0:T(8,128)(2,1)S(1)} copy-done((bf16[1,2048,512]{2,1,0:T(8,128)(2,1)S(1)}, bf16[1,2048,512]{2,1,0:T(8,128)(2,1)}, u32[]{:S(2)}) %copy-start) | copy-done | bytes 2097176
  3.3 0.0 copy-start.1
  3.3 0.9 copy-done.1
  4.2 0.0 copy-start.2
  4.2 0.7 copy-done.2
  4.9 115.6 %moe.1 = bf16[512,128]{1,0:T(8,128)(2,1)S(1)} custom-call(bf16[512,128]{1,0:T(8,128)(2,1)S(1)} %copy-done.1, f32[1,2048]{1,0:T(1,128)S(1)} %bitcast.1, bf16[1,2048,512]{2,1,0:T(8,128)(2,1)S(1)} %copy-done, bf16[1,2048,512]{2,1,0:T(8,128)(2,1)} %up_hbm.1, bf16[1,512,2048]{2,1,0:T(8,128)(2,1)} %down_hbm.1, s32[512,2]{1,0:T(8,128)S(1)} %copy.8.ids_hbm, ...), custom_call_target="tpu_custom_call" | custom-call | tf_op jit(solution)/shard_map/moe/pallas_call | solution.py:305
  120.5 0.7 copy.11
Async XLA Ops:
  1.7 1.6 %copy-start = (bf16[1,2048,512]{2,1,0:T(8,128)(2,1)S(1)}, bf16[1,2048,512]{2,1,0:T(8,128)(2,1)}, u32[]{:S(2)}) copy-start(bf16[1,2048,512]{2,1,0:T(8,128)(2,1)} %gate_hbm.1) | copy-start | bytes 6291460
  3.3 0.9 copy-start.1
  4.2 0.7 copy-start.2

commit v2 on v1

v2 whole, which is shorter than its diff:
```python
from functools import partial

import jax
import jax.numpy as jnp
from jax import lax
from jax.experimental import pallas as pl
from jax.experimental.pallas import tpu as pltpu
from jax.sharding import PartitionSpec as P

MESH = pl.DeviceIdType.MESH
F32 = jnp.float32
BF16 = jnp.bfloat16
CHIPS = 4
EPG = 8
SLOTS = 8
ORDER = ('D0', 'H3', 'D1', 'S0', 'S1', 'E0', 'E1', 'C1', 'C0')
NB = 2


def dot(a, b, contract=((1,), (0,))):
    return lax.dot_general(a, b, (contract, ((), ())), preferred_element_type=F32)


def to_row(col):
    n = col.shape[0]
    eye = lax.broadcasted_iota(jnp.int32, (n, n), 0) == lax.broadcasted_iota(jnp.int32, (n, n), 1)
    return jnp.sum(jnp.where(eye, col, jnp.zeros_like(col)), axis=0, keepdims=True)


def body(
    ep_count, tp_count,
    tokens, gain_hbm, gate_hbm, up_hbm, down_hbm, ids_hbm, wts_hbm,
    out,
    tok_v, xin, gain, ids, wts, gate, up, down, xn, sb, rbuf, sbuf, xe, yo, pbuf, obuf, ret, mx,
    known, w_sem, in_sem, tp_send, tp_recv, s1, r1, s2, r2, s3, r3, s4, r4, fin_send, fin_recv,
):
    e = lax.axis_index("ep")
    t = lax.axis_index("tp")
    groups = ep_count // EPG
    chips = ep_count // 2
    half = groups // 2
    c = lax.rem(e, 2)
    z = e // 2
    p = lax.rem(z, CHIPS)
    g = z // CHIPS
    rows = xn.shape[0]
    width = gate.shape[0]
    my_e = 2 * p + c

    weight_copies = [
        pltpu.make_async_copy(gate_hbm.at[0], gate, w_sem.at[0]),
        pltpu.make_async_copy(up_hbm.at[0], up, w_sem.at[1]),
        pltpu.make_async_copy(down_hbm.at[0], down, w_sem.at[2]),
    ]
    small_copies = [
        pltpu.make_async_copy(ids_hbm, ids, in_sem.at[0]),
        pltpu.make_async_copy(wts_hbm, wts, in_sem.at[1]),
        pltpu.make_async_copy(tokens, tok_v, in_sem.at[2]),
        pltpu.make_async_copy(gain_hbm, gain, in_sem.at[3]),
    ]
    for cp in small_copies:
        cp.start()
    barrier = pltpu.get_barrier_semaphore()

    def column(zz):
        return {"ep": lax.rem(zz + 2 * chips, chips) * 2 + c}

    for peer in ({"ep": z * 2 + 1 - c}, column(z + 1), column(z - 1)):
        pl.semaphore_signal(barrier, inc=1, device_id=peer, device_id_type=MESH)

    if tp_count > 1:
        @pl.loop(1, tp_count)
        def _(k):
            pl.semaphore_signal(barrier, inc=1, device_id={"tp": lax.rem(t + k, tp_count)}, device_id_type=MESH)

    for cp in weight_copies:
        cp.start()

    for cp in small_copies[:2]:
        cp.wait()
    tok = ids.shape[1]
    pick = lax.broadcasted_iota(jnp.int32, (rows, tok), 1) == (
        lax.broadcasted_iota(jnp.int32, (rows, tok), 0) + t * rows
    )
    id_col = [jnp.sum(jnp.where(pick, ids[k:k + 1, :], 0), axis=1, keepdims=True) for k in range(2)]
    w_col = [jnp.sum(jnp.where(pick, wts[k:k + 1, :], 0.0), axis=1, keepdims=True) for k in range(2)]
    id_row = [to_row(v) for v in id_col]
    before = lax.broadcasted_iota(jnp.int32, (rows, rows), 1) < lax.broadcasted_iota(jnp.int32, (rows, rows), 0)
    g_col = id_col[0] // EPG
    same = before & ((id_row[0] // EPG) == g_col)
    rank = jnp.sum(jnp.where(same, 1, 0), axis=1, keepdims=True)
    rel = lax.rem(g_col - g + groups, groups)
    target = rel * SLOTS + rank
    q_col = []
    for k in range(2):
        hit = jnp.where(id_row[0] == id_col[k], 1, 0) + jnp.where(id_row[1] == id_col[k], 1, 0)
        q_col.append(jnp.sum(jnp.where(before, hit, 0), axis=1, keepdims=True))
    lane = lax.broadcasted_iota(jnp.int32, (rows, 128), 1)
    lane_lo = lax.rem(lane, 64)
    w_tok = jnp.zeros((rows, 128), F32)
    for k in range(2):
        high = w_col[k].astype(BF16).astype(F32)
        part = jnp.where(lane < 64, high, w_col[k] - high)
        on = (lane_lo // 8 == lax.rem(id_col[k], EPG)) & (lax.rem(lane, 2) == q_col[k])
        w_tok = w_tok + jnp.where(on, part, 0.0)
    xn[:, width:] = w_tok.astype(BF16)
    place = jnp.where(
        lax.broadcasted_iota(jnp.int32, (groups * SLOTS, rows), 0) == to_row(target), 1.0, 0.0
    ).astype(BF16)
    unplace = jnp.where(
        lax.broadcasted_iota(jnp.int32, (rows, groups * SLOTS), 1) == target, 1.0, 0.0
    ).astype(BF16)

    for cp in small_copies[2:]:
        cp.wait()
    xin[t] = tok_v[pl.ds(pl.multiple_of(t * rows, rows), rows), :]
    pl.semaphore_wait(barrier, 3 + (tp_count - 1))

    if tp_count > 1:
        @pl.loop(1, tp_count)
        def _(k):
            peer = lax.rem(t + k, tp_count)
            pltpu.make_async_remote_copy(
                src_ref=tok_v.at[pl.ds(peer * rows, rows)], dst_ref=xin.at[t],
                send_sem=tp_send, recv_sem=tp_recv, device_id={"tp": peer}, device_id_type=MESH,
            ).start()

    def tell(i):
        for side in range(2):
            pl.semaphore_signal(
                known.at[2 * i + side], inc=1, device_id=column(z + (1 - 2 * side) * 2**i), device_id_type=MESH
            )

    def hear(i):
        for side in range(2):
            pl.semaphore_wait(known.at[2 * i + side], 1)

    for i in range(3):
        tell(i)
        hear(i)
    tell(3)
    if tp_count > 1:
        pltpu.make_async_copy(xin.at[pl.ds(0, tp_count - 1)], xin.at[pl.ds(0, tp_count - 1)], tp_recv).wait()
    piece = xin.shape[2]
    total = jnp.zeros((rows, piece), F32)
    for i in range(tp_count):
        v = xin[i].astype(F32)
        total = total + v * v
    scale = lax.rsqrt(jnp.sum(total, axis=1, keepdims=True) / width + 1e-06)
    for i in range(tp_count):
        cols = slice(i * piece, (i + 1) * piece)
        xn[:, cols] = (xin[i].astype(F32) * scale * gain[:, cols]).astype(BF16)
    placed = dot(place, xn[...])
    for r in range(groups):
        sb[r] = placed[r * SLOTS:(r + 1) * SLOTS].astype(BF16)

    def ep_of(zz):
        return {"ep": zz * 2 + c}

    def send1(r, dest_z, k, b):
        return pltpu.make_async_remote_copy(
            src_ref=sb.at[r], dst_ref=rbuf.at[k, b], send_sem=s1.at[k], recv_sem=r1.at[k],
            device_id=ep_of(dest_z), device_id_type=MESH,
        )

    odd = lax.rem(p, 2)

    def dispatch(k):
        if k == 1:
            send1(half, lax.rem(g + half, groups) * CHIPS + 2 * (1 - p // 2) + odd, k, 2).start()
            pltpu.make_async_copy(sb.at[0], rbuf.at[k, 3], r1.at[k]).start()
        for d in (2, 1) if k == 0 else (3,):
            b = 2 * ((d - 1) % 2) + odd
            send1(d, lax.rem(g + d, groups) * CHIPS + p // 2, k, b).start()
            send1(groups - d, lax.rem(g + groups - d, groups) * CHIPS + 2 + p // 2, k, b).start()

    def dispatched(k):
        n = 4 if k == 0 else 3
        pltpu.make_async_copy(sb.at[pl.ds(0, n)], sb.at[pl.ds(0, n)], s1.at[k]).wait()

    row_of = lax.broadcasted_iota(jnp.int32, (32, 64), 0) // SLOTS
    lane_of = lax.rem(lax.broadcasted_iota(jnp.int32, (32, 64), 1) // 2, 4)
    diagonal = row_of == lane_of

    def select(k):
        pltpu.make_async_copy(rbuf.at[k], rbuf.at[k], r1.at[k]).wait()
        got = rbuf[k].reshape(4 * SLOTS, width + 128)
        wide = got[:, width:width + 64].astype(F32)
        sel = jnp.where(diagonal & (wide != 0.0), 1.0, 0.0).astype(BF16)
        chosen = dot(sel, got[:, :width], ((0,), (0,)))
        for ee in range(EPG):
            sbuf[k, ee] = chosen[ee * 8:(ee + 1) * 8].astype(BF16)
        for d in range(1, EPG):
            ee = lax.rem(my_e + d, EPG)
            pltpu.make_async_remote_copy(
                src_ref=sbuf.at[k, ee], dst_ref=xe.at[k, my_e], send_sem=s2, recv_sem=r2.at[k],
                device_id={"ep": g * EPG + ee}, device_id_type=MESH,
            ).start()
        pltpu.make_async_copy(sbuf.at[k, my_e], xe.at[k, my_e], r2.at[k]).start()

    def expert(k):
        pltpu.make_async_copy(xe.at[k], xe.at[k], r2.at[k]).wait()
        x = xe[k].reshape(64, width)
        a = dot(x, gate[...])
        b = dot(x, up[...])
        h = (a / (1.0 + jnp.exp(-a)) * b).astype(BF16)
        y = dot(h, down[...])
        for i in range(EPG):
            yo[k, i] = y[i * 8:(i + 1) * 8].astype(BF16)
        for d in range(1, EPG):
            ee = lax.rem(my_e + d, EPG)
            pltpu.make_async_remote_copy(
                src_ref=yo.at[k, ee], dst_ref=pbuf.at[k, my_e], send_sem=s3, recv_sem=r3.at[k],
                device_id={"ep": g * EPG + ee}, device_id_type=MESH,
            ).start()
        pltpu.make_async_copy(yo.at[k, my_e], pbuf.at[k, my_e], r3.at[k]).start()

    def combine(k):
        pltpu.make_async_copy(pbuf.at[k], pbuf.at[k], r3.at[k]).wait()
        parts = pbuf[k].reshape(64, width)
        wide = rbuf[k].reshape(4 * SLOTS, width + 128)[:, width:].astype(F32)
        high = jnp.where(diagonal, wide[:, :64], 0.0).astype(BF16)
        low = jnp.where(diagonal, wide[:, 64:], 0.0).astype(BF16)
        y = dot(high, parts) + dot(low, parts)
        for b in range(4):
            obuf[k, b] = y[b * 8:(b + 1) * 8].astype(BF16)
        sign = 1 - 2 * (p // 2)

        def back(b, src_z, r):
            pltpu.make_async_remote_copy(
                src_ref=obuf.at[k, b], dst_ref=ret.at[r], send_sem=s4, recv_sem=r4,
                device_id=ep_of(src_z), device_id_type=MESH,
            ).start()

        for d in (2, 1) if k == 0 else (3,):
            for i in range(2):
                back(
                    2 * ((d - 1) % 2) + i,
                    lax.rem(g + groups - sign * d, groups) * CHIPS + 2 * odd + i,
                    lax.rem(groups + sign * d, groups),
                )
        if k == 1:
            back(2, lax.rem(g + half, groups) * CHIPS + lax.rem(p + 2, CHIPS), half)
            pltpu.make_async_copy(obuf.at[k, 3], ret.at[0], r4).start()

    for cp in weight_copies:
        cp.wait()
    phases = {"H": hear, "D": dispatch, "W": dispatched, "S": select, "E": expert, "C": combine}
    for step in ORDER:
        phases[step[0]](int(step[1]))

    pltpu.make_async_copy(ret, ret, r4).wait()
    mixed = dot(unplace, ret[...].reshape(groups * SLOTS, width))
    for i in range(tp_count):
        mx[i] = mixed[:, i * piece:(i + 1) * piece].astype(BF16)
    mine = pltpu.make_async_copy(mx.at[t], out.at[pl.ds(t * rows, rows)], in_sem.at[2])
    mine.start()
    if tp_count > 1:
        @pl.loop(1, tp_count)
        def _(k):
            peer = lax.rem(t + k, tp_count)
            pltpu.make_async_remote_copy(
                src_ref=mx.at[peer], dst_ref=out.at[pl.ds(t * rows, rows)],
                send_sem=fin_send, recv_sem=fin_recv, device_id={"tp": peer}, device_id_type=MESH,
            ).start()

        others = mx.at[pl.ds(0, tp_count - 1)]
        pltpu.make_async_copy(others, others, fin_recv).wait()
        pltpu.make_async_copy(others, others, fin_send).wait()
        others = xin.at[pl.ds(0, tp_count - 1)]
        pltpu.make_async_copy(others, others, tp_send).wait()
    mine.wait()

    for k in range(NB):
        if "W%d" % k not in ORDER:
            dispatched(k)
    for src, sem in ((sbuf, s2), (yo, s3)):
        every = src.at[:, pl.ds(0, EPG - 1)]
        pltpu.make_async_copy(every, every, sem).wait()
    every = ret.at[pl.ds(0, groups - 1)]
    pltpu.make_async_copy(every, every, s4).wait()


def local(tokens, norm_gain, gate_weight, up_weight, down_weight, expert_ids, route_weight, ep_count, tp_count):
    tok, piece = tokens.shape
    rows = tok // tp_count
    _, width, ff = gate_weight.shape
    groups = ep_count // EPG
    nb = NB
    wide = width + 128
    any_spec = pl.BlockSpec(memory_space=pl.ANY)
    dma = pltpu.SemaphoreType.DMA
    return pl.pallas_call(
        partial(body, ep_count, tp_count),
        out_shape=jax.ShapeDtypeStruct(tokens.shape, BF16),
        in_specs=[any_spec] * 7,
        out_specs=any_spec,
        scratch_shapes=[
            pltpu.VMEM((tok, piece), BF16),
            pltpu.VMEM((tp_count, rows, piece), BF16),
            pltpu.VMEM((1, width), F32),
            pltpu.VMEM((2, tok), jnp.int32),
            pltpu.VMEM((2, tok), F32),
            pltpu.VMEM((width, ff), BF16),
            pltpu.VMEM((width, ff), BF16),
            pltpu.VMEM((ff, width), BF16),
            pltpu.VMEM((rows, wide), BF16),
            pltpu.VMEM((groups, SLOTS, wide), BF16),
            pltpu.VMEM((nb, 4, SLOTS, wide), BF16),
            pltpu.VMEM((nb, EPG, 8, width), BF16),
            pltpu.VMEM((nb, EPG, 8, width), BF16),
            pltpu.VMEM((nb, EPG, 8, width), BF16),
            pltpu.VMEM((nb, EPG, 8, width), BF16),
            pltpu.VMEM((nb, 4, SLOTS, width), BF16),
            pltpu.VMEM((groups, SLOTS, width), BF16),
            pltpu.VMEM((tp_count, rows, piece), BF16),
            pltpu.SemaphoreType.REGULAR((8,)),
            dma((3,)), dma((4,)), dma, dma,
            dma((nb,)), dma((nb,)), dma, dma((nb,)), dma, dma((nb,)), dma, dma, dma, dma,
        ],
        compiler_params=pltpu.CompilerParams(
            collective_id=0, has_side_effects=True, vmem_limit_bytes=67043328
        ),
        name="moe",
    )(tokens, norm_gain.reshape(1, width), gate_weight, up_weight, down_weight, expert_ids.T, route_weight.T)


def solution(mesh):
    in_specs = (
        P("ep", "tp"),
        P(),
        P("ep", None, None),
        P("ep", None, None),
        P("ep", None, None),
        P("ep", None),
        P("ep", None),
    )
    fn = partial(local, ep_count=mesh.shape["ep"], tp_count=mesh.shape["tp"])
    return jax.shard_map(fn, mesh=mesh, in_specs=in_specs, out_specs=P("ep", "tp"), check_vma=False)
```

time: 121 us -> 110 us (0.909)
  Pallas kernels: 116 us -> 108 us
  local copies, waits for them, and re-layouts: 5.5 us -> 1.57 us
    pallas_call x1, Pallas kernels: 116 us -> 108 us  [local(): pl.pallas_call(partial(body, ep_count, tp_count), out_shape=jax.ShapeDtyp...]
    unnamed x9 -> x1, local copies, waits for them, and re-layouts: 5.5 us -> 1.57 us
where the time goes in v2:
time: 110 us; the launch traced here: 109 us
  Pallas kernels  108 us (98%)
  local copies, waits for them, and re-layouts  1.57 us (1%)
    pallas_call x1, Pallas kernels, local(): pl.pallas_call(partial(body, ep_count, tp_count), out_shape=jax.ShapeDtyp...  108 us

profile of v2, /device:TPU:1, one launch (start us, length us, event | category | flops | bytes accessed | tf_op | source)
XLA Modules:
  0.0 109.3 jit_solution(15365654565210111818)
XLA Ops:
  0.0 107.7 %moe.1 = bf16[512,128]{1,0:T(8,128)(2,1)} custom-call(bf16[512,128]{1,0:T(8,128)(2,1)} %tokens.1, f32[1,2048]{1,0:T(1,128)} %bitcast.3, bf16[1,2048,512]{2,1,0:T(8,128)(2,1)} %gate_hbm.1, bf16[1,2048,512]{2,1,0:T(8,128)(2,1)} %up_hbm.1, bf16[1,512,2048]{2,1,0:T(8,128)(2,1)} %down_hbm.1, s32[2,512]{1,0:T(2,128)} %bitcast.4, f32[2,512]{1,0:T(2,128)} %bitcast.5), custom_call_target="tpu_custom_call" | custom-call | tf_op jit(solution)/shard_map/moe/pallas_call | solution.py:293
  107.7 1.6 %copy.9 = bf16[512,128]{1,0:T(8,128)(2,1)} copy(bf16[512,128]{1,0:T(8,128)(2,1)} %moe.1) | data formatting | bytes 262144

commit v3 on v2

--- a/solution.py
+++ b/solution.py
@@ -13,8 +13,20 @@
 CHIPS = 4
 EPG = 8
 SLOTS = 8
-ORDER = ('D0', 'H3', 'D1', 'S0', 'S1', 'E0', 'E1', 'C1', 'C0')
+ORDER = ('D0', 'H3', 'D1', 'S0', 'S1', 'E0', 'E1', 'C0', 'A0', 'C1', 'A1', 'X1', 'X0')
+RETURNS = {
+    'A0': ((0,), 0, 4, True),
+    'A1': ((1,), 0, 4, True),
+    'B0': ((0,), 4, 12, True),
+    'B1': ((1,), 4, 12, True),
+    'G0': ((0,), 12, 32, True),
+    'G1': ((1,), 12, 32, True),
+    'W': ((0, 1), 0, 32, False),
+    'X0': ((0,), 4, 32, True),
+    'X1': ((1,), 4, 32, True),
+}
 NB = 2
+HOPS = (1, 2, 4, 6)
 
 
 def dot(a, b, contract=((1,), (0,))):
@@ -128,7 +140,7 @@
     def tell(i):
         for side in range(2):
             pl.semaphore_signal(
-                known.at[2 * i + side], inc=1, device_id=column(z + (1 - 2 * side) * 2**i), device_id_type=MESH
+                known.at[2 * i + side], inc=1, device_id=column(z + (1 - 2 * side) * HOPS[i]), device_id_type=MESH
             )
 
     def hear(i):
@@ -164,6 +176,9 @@
         )
 
     odd = lax.rem(p, 2)
+    top = p // 2
+    peers = [2 * chip + core for chip in (3 * (1 - top), 2 - top, 1 + 4 * top - p) for core in (0, 1)]
+    peers.append(my_e + 1 - 2 * c)
 
     def dispatch(k):
         if k == 1:
@@ -190,8 +205,7 @@
         chosen = dot(sel, got[:, :width], ((0,), (0,)))
         for ee in range(EPG):
             sbuf[k, ee] = chosen[ee * 8:(ee + 1) * 8].astype(BF16)
-        for d in range(1, EPG):
-            ee = lax.rem(my_e + d, EPG)
+        for ee in peers:
             pltpu.make_async_remote_copy(
                 src_ref=sbuf.at[k, ee], dst_ref=xe.at[k, my_e], send_sem=s2, recv_sem=r2.at[k],
                 device_id={"ep": g * EPG + ee}, device_id_type=MESH,
@@ -207,8 +221,7 @@
         y = dot(h, down[...])
         for i in range(EPG):
             yo[k, i] = y[i * 8:(i + 1) * 8].astype(BF16)
-        for d in range(1, EPG):
-            ee = lax.rem(my_e + d, EPG)
+        for ee in peers:
             pltpu.make_async_remote_copy(
                 src_ref=yo.at[k, ee], dst_ref=pbuf.at[k, my_e], send_sem=s3, recv_sem=r3.at[k],
                 device_id={"ep": g * EPG + ee}, device_id_type=MESH,
@@ -224,30 +237,42 @@
         y = dot(high, parts) + dot(low, parts)
         for b in range(4):
             obuf[k, b] = y[b * 8:(b + 1) * 8].astype(BF16)
+        if k == 1:
+            pltpu.make_async_copy(obuf.at[k, 3], ret.at[0], r4).start()
+
+    def returns():
         sign = 1 - 2 * (p // 2)
-
-        def back(b, src_z, r):
-            pltpu.make_async_remote_copy(
-                src_ref=obuf.at[k, b], dst_ref=ret.at[r], send_sem=s4, recv_sem=r4,
-                device_id=ep_of(src_z), device_id_type=MESH,
-            ).start()
-
-        for d in (2, 1) if k == 0 else (3,):
+        found = []
+        for d in (1, 2, 3):
             for i in range(2):
-                back(
-                    2 * ((d - 1) % 2) + i,
-                    lax.rem(g + groups - sign * d, groups) * CHIPS + 2 * odd + i,
-                    lax.rem(groups + sign * d, groups),
-                )
-        if k == 1:
-            back(2, lax.rem(g + half, groups) * CHIPS + lax.rem(p + 2, CHIPS), half)
-            pltpu.make_async_copy(obuf.at[k, 3], ret.at[0], r4).start()
+                src_z = lax.rem(g + groups - sign * d, groups) * CHIPS + 2 * odd + i
+                found.append(((d - 1) // 2, 2 * ((d - 1) % 2) + i, src_z, lax.rem(groups + sign * d, groups)))
+        found.append((1, 2, lax.rem(g + half, groups) * CHIPS + lax.rem(p + 2, CHIPS), half))
+        return found
+
+    def give(name):
+        ks, low, high, act = RETURNS[name]
+        for k, b, src_z, r in returns():
+            if k in ks:
+                @pl.when((src_z >= low) & (src_z < high))
+                def _():
+                    cp = pltpu.make_async_remote_copy(
+                        src_ref=obuf.at[k, b], dst_ref=ret.at[r], send_sem=s4.at[k, b], recv_sem=r4,
+                        device_id=ep_of(src_z), device_id_type=MESH,
+                    )
+                    if act:
+                        cp.start()
+                    else:
+                        cp.wait_send()
 
     for cp in weight_copies:
         cp.wait()
     phases = {"H": hear, "D": dispatch, "W": dispatched, "S": select, "E": expert, "C": combine}
     for step in ORDER:
-        phases[step[0]](int(step[1]))
+        if step in RETURNS:
+            give(step)
+        else:
+            phases[step[0]](int(step[1]))
 
     pltpu.make_async_copy(ret, ret, r4).wait()
     mixed = dot(unplace, ret[...].reshape(groups * SLOTS, width))
@@ -274,11 +299,10 @@
     for k in range(NB):
         if "W%d" % k not in ORDER:
             dispatched(k)
+    give("W")
     for src, sem in ((sbuf, s2), (yo, s3)):
         every = src.at[:, pl.ds(0, EPG - 1)]
         pltpu.make_async_copy(every, every, sem).wait()
-    every = ret.at[pl.ds(0, groups - 1)]
-    pltpu.make_async_copy(every, every, s4).wait()
 
 
 def local(tokens, norm_gain, gate_weight, up_weight, down_weight, expert_ids, route_weight, ep_count, tp_count):
@@ -316,7 +340,7 @@
             pltpu.VMEM((tp_count, rows, piece), BF16),
             pltpu.SemaphoreType.REGULAR((8,)),
             dma((3,)), dma((4,)), dma, dma,
-            dma((nb,)), dma((nb,)), dma, dma((nb,)), dma, dma((nb,)), dma, dma, dma, dma,
+            dma((nb,)), dma((nb,)), dma, dma((nb,)), dma, dma((nb,)), dma((nb, 4)), dma, dma, dma,
         ],
         compiler_params=pltpu.CompilerParams(
             collective_id=0, has_side_effects=True, vmem_limit_bytes=67043328

time: 110 us -> 104 us (0.945)
  the two profiles are of different devices: /device:TPU:1 before, /device:TPU:160 now
where the time goes in v3:
time: 104 us
  Pallas kernels  102 us (98%)
  local copies, waits for them, and re-layouts  1.57 us (2%)
    pallas_call x1, Pallas kernels, local(): pl.pallas_call(partial(body, ep_count, tp_count), out_shape=jax.ShapeDtyp...  102 us

profile of v3, /device:TPU:160, one launch (start us, length us, event | category | flops | bytes accessed | tf_op | source)
XLA Modules:
  0.0 103.8 jit_solution(17748307702125547376)
XLA Ops:
  0.0 102.2 %moe.1 = bf16[512,128]{1,0:T(8,128)(2,1)} custom-call(bf16[512,128]{1,0:T(8,128)(2,1)} %tokens.1, f32[1,2048]{1,0:T(1,128)} %bitcast.3, bf16[1,2048,512]{2,1,0:T(8,128)(2,1)} %gate_hbm.1, bf16[1,2048,512]{2,1,0:T(8,128)(2,1)} %up_hbm.1, bf16[1,512,2048]{2,1,0:T(8,128)(2,1)} %down_hbm.1, s32[2,512]{1,0:T(2,128)} %bitcast.4, f32[2,512]{1,0:T(2,128)} %bitcast.5), custom_call_target="tpu_custom_call" | custom-call | tf_op jit(solution)/shard_map/moe/pallas_call | solution.py:317
  102.3 1.6 %copy.9 = bf16[512,128]{1,0:T(8,128)(2,1)} copy(bf16[512,128]{1,0:T(8,128)(2,1)} %moe.1) | data formatting | bytes 262144

commit v4 on v3

--- a/solution.py
+++ b/solution.py
@@ -44,7 +44,7 @@
     tokens, gain_hbm, gate_hbm, up_hbm, down_hbm, ids_hbm, wts_hbm,
     out,
     tok_v, xin, gain, ids, wts, gate, up, down, xn, sb, rbuf, sbuf, xe, yo, pbuf, obuf, ret, mx,
-    known, w_sem, in_sem, tp_send, tp_recv, s1, r1, s2, r2, s3, r3, s4, r4, fin_send, fin_recv,
+    wsend, wrecv, wmat, known, sw, rw, w_sem, in_sem, tp_send, tp_recv, s1, r1, s2, r2, s3, r3, s4, r4, fin_send, fin_recv,
 ):
     e = lax.axis_index("ep")
     t = lax.axis_index("tp")
@@ -108,14 +108,18 @@
         hit = jnp.where(id_row[0] == id_col[k], 1, 0) + jnp.where(id_row[1] == id_col[k], 1, 0)
         q_col.append(jnp.sum(jnp.where(before, hit, 0), axis=1, keepdims=True))
     lane = lax.broadcasted_iota(jnp.int32, (rows, 128), 1)
-    lane_lo = lax.rem(lane, 64)
     w_tok = jnp.zeros((rows, 128), F32)
     for k in range(2):
-        high = w_col[k].astype(BF16).astype(F32)
-        part = jnp.where(lane < 64, high, w_col[k] - high)
-        on = (lane_lo // 8 == lax.rem(id_col[k], EPG)) & (lax.rem(lane, 2) == q_col[k])
-        w_tok = w_tok + jnp.where(on, part, 0.0)
-    xn[:, width:] = w_tok.astype(BF16)
+        on = lane == rank * 16 + lax.rem(id_col[k], EPG) * 2 + q_col[k]
+        w_tok = w_tok + jnp.where(on, w_col[k], 0.0)
+    w_high = w_tok.astype(BF16)
+    w_low = (w_tok - w_high.astype(F32)).astype(BF16)
+    of_group = jnp.where(
+        lax.broadcasted_iota(jnp.int32, (groups, rows), 0) == to_row(rel), 1.0, 0.0
+    ).astype(BF16)
+    table = dot(of_group, w_high) + dot(of_group, w_low)
+    for r in range(groups):
+        wsend[r] = table[r:r + 1]
     place = jnp.where(
         lax.broadcasted_iota(jnp.int32, (groups * SLOTS, rows), 0) == to_row(target), 1.0, 0.0
     ).astype(BF16)
@@ -175,34 +179,58 @@
             device_id=ep_of(dest_z), device_id_type=MESH,
         )
 
+    def sendw(r, dest_z, k, b):
+        return pltpu.make_async_remote_copy(
+            src_ref=wsend.at[r], dst_ref=wrecv.at[k, b], send_sem=sw.at[k], recv_sem=rw.at[k],
+            device_id=ep_of(dest_z), device_id_type=MESH,
+        )
+
     odd = lax.rem(p, 2)
     top = p // 2
     peers = [2 * chip + core for chip in (3 * (1 - top), 2 - top, 1 + 4 * top - p) for core in (0, 1)]
     peers.append(my_e + 1 - 2 * c)
 
     def dispatch(k):
+        plan = []
         if k == 1:
-            send1(half, lax.rem(g + half, groups) * CHIPS + 2 * (1 - p // 2) + odd, k, 2).start()
+            plan.append((half, lax.rem(g + half, groups) * CHIPS + 2 * (1 - p // 2) + odd, 2))
             pltpu.make_async_copy(sb.at[0], rbuf.at[k, 3], r1.at[k]).start()
+            pltpu.make_async_copy(wsend.at[0], wrecv.at[k, 3], rw.at[k]).start()
         for d in (2, 1) if k == 0 else (3,):
             b = 2 * ((d - 1) % 2) + odd
-            send1(d, lax.rem(g + d, groups) * CHIPS + p // 2, k, b).start()
-            send1(groups - d, lax.rem(g + groups - d, groups) * CHIPS + 2 + p // 2, k, b).start()
+            plan.append((d, lax.rem(g + d, groups) * CHIPS + p // 2, b))
+            plan.append((groups - d, lax.rem(g + groups - d, groups) * CHIPS + 2 + p // 2, b))
+        for send in (sendw, send1):
+            for r, dest_z, b in plan:
+                send(r, dest_z, k, b).start()
 
     def dispatched(k):
         n = 4 if k == 0 else 3
         pltpu.make_async_copy(sb.at[pl.ds(0, n)], sb.at[pl.ds(0, n)], s1.at[k]).wait()
+        pltpu.make_async_copy(wsend.at[pl.ds(0, n)], wsend.at[pl.ds(0, n)], sw.at[k]).wait()
 
     row_of = lax.broadcasted_iota(jnp.int32, (32, 64), 0) // SLOTS
     lane_of = lax.rem(lax.broadcasted_iota(jnp.int32, (32, 64), 1) // 2, 4)
     diagonal = row_of == lane_of
+    slot_of = lax.rem(lax.broadcasted_iota(jnp.int32, (32, 128), 0), SLOTS)
+    in_slot = lax.broadcasted_iota(jnp.int32, (32, 128), 1) // 16 == slot_of
+    wide_row = lax.rem(lax.broadcasted_iota(jnp.int32, (128, 64), 0), 16)
+    wide_lane = lax.broadcasted_iota(jnp.int32, (128, 64), 1)
+    spread = jnp.where(wide_row == wide_lane // 8 * 2 + lax.rem(wide_lane, 2), 1.0, 0.0).astype(BF16)
 
     def select(k):
         pltpu.make_async_copy(rbuf.at[k], rbuf.at[k], r1.at[k]).wait()
-        got = rbuf[k].reshape(4 * SLOTS, width + 128)
-        wide = got[:, width:width + 64].astype(F32)
-        sel = jnp.where(diagonal & (wide != 0.0), 1.0, 0.0).astype(BF16)
-        chosen = dot(sel, got[:, :width], ((0,), (0,)))
+        pltpu.make_async_copy(wrecv.at[k], wrecv.at[k], rw.at[k]).wait()
+        weights = jnp.concatenate([jnp.broadcast_to(wrecv[k, b], (SLOTS, 128)) for b in range(4)], axis=0)
+        weights = jnp.where(in_slot, weights, 0.0)
+        w_hi = weights.astype(BF16)
+        w_lo = (weights - w_hi.astype(F32)).astype(BF16)
+        high = jnp.where(diagonal, dot(w_hi, spread), 0.0)
+        low = jnp.where(diagonal, dot(w_lo, spread), 0.0)
+        wmat[k, 0] = high.astype(BF16)
+        wmat[k, 1] = low.astype(BF16)
+        sel = jnp.where(high != 0.0, 1.0, 0.0).astype(BF16)
+        chosen = dot(sel, rbuf[k].reshape(4 * SLOTS, width), ((0,), (0,)))
         for ee in range(EPG):
             sbuf[k, ee] = chosen[ee * 8:(ee + 1) * 8].astype(BF16)
         for ee in peers:
@@ -231,10 +259,7 @@
     def combine(k):
         pltpu.make_async_copy(pbuf.at[k], pbuf.at[k], r3.at[k]).wait()
         parts = pbuf[k].reshape(64, width)
-        wide = rbuf[k].reshape(4 * SLOTS, width + 128)[:, width:].astype(F32)
-        high = jnp.where(diagonal, wide[:, :64], 0.0).astype(BF16)
-        low = jnp.where(diagonal, wide[:, 64:], 0.0).astype(BF16)
-        y = dot(high, parts) + dot(low, parts)
+        y = dot(wmat[k, 0], parts) + dot(wmat[k, 1], parts)
         for b in range(4):
             obuf[k, b] = y[b * 8:(b + 1) * 8].astype(BF16)
         if k == 1:
@@ -311,7 +336,6 @@
     _, width, ff = gate_weight.shape
     groups = ep_count // EPG
     nb = NB
-    wide = width + 128
     any_spec = pl.BlockSpec(memory_space=pl.ANY)
     dma = pltpu.SemaphoreType.DMA
     return pl.pallas_call(
@@ -328,9 +352,9 @@
             pltpu.VMEM((width, ff), BF16),
             pltpu.VMEM((width, ff), BF16),
             pltpu.VMEM((ff, width), BF16),
-            pltpu.VMEM((rows, wide), BF16),
-            pltpu.VMEM((groups, SLOTS, wide), BF16),
-            pltpu.VMEM((nb, 4, SLOTS, wide), BF16),
+            pltpu.VMEM((rows, width), BF16),
+            pltpu.VMEM((groups, SLOTS, width), BF16),
+            pltpu.VMEM((nb, 4, SLOTS, width), BF16),
             pltpu.VMEM((nb, EPG, 8, width), BF16),
             pltpu.VMEM((nb, EPG, 8, width), BF16),
             pltpu.VMEM((nb, EPG, 8, width), BF16),
@@ -338,7 +362,11 @@
             pltpu.VMEM((nb, 4, SLOTS, width), BF16),
             pltpu.VMEM((groups, SLOTS, width), BF16),
             pltpu.VMEM((tp_count, rows, piece), BF16),
+            pltpu.VMEM((groups, 1, 128), F32),
+            pltpu.VMEM((nb, 4, 1, 128), F32),
+            pltpu.VMEM((nb, 2, 32, 64), BF16),
             pltpu.SemaphoreType.REGULAR((8,)),
+            dma((nb,)), dma((nb,)),
             dma((3,)), dma((4,)), dma, dma,
             dma((nb,)), dma((nb,)), dma, dma((nb,)), dma, dma((nb,)), dma((nb, 4)), dma, dma, dma,
         ],

time: 104 us -> 103 us (level)
    pallas_call x1, Pallas kernels: 102 us -> 101 us  [local(): pl.pallas_call(partial(body, ep_count, tp_count), out_shape=jax.ShapeDtyp...]
where the time goes in v4:
time: 103 us; the launch traced here: 102 us
  Pallas kernels  101 us (98%)
  local copies, waits for them, and re-layouts  1.57 us (2%)
    pallas_call x1, Pallas kernels, local(): pl.pallas_call(partial(body, ep_count, tp_count), out_shape=jax.ShapeDtyp...  101 us

profile of v4, /device:TPU:160, one launch (start us, length us, event | category | flops | bytes accessed | tf_op | source)
XLA Modules:
  0.0 102.5 jit_solution(10037255003869379042)
XLA Ops:
  0.0 100.9 %moe.1 = bf16[512,128]{1,0:T(8,128)(2,1)} custom-call(bf16[512,128]{1,0:T(8,128)(2,1)} %tokens.1, f32[1,2048]{1,0:T(1,128)} %bitcast.3, bf16[1,2048,512]{2,1,0:T(8,128)(2,1)} %gate_hbm.1, bf16[1,2048,512]{2,1,0:T(8,128)(2,1)} %up_hbm.1, bf16[1,512,2048]{2,1,0:T(8,128)(2,1)} %down_hbm.1, s32[2,512]{1,0:T(2,128)} %bitcast.4, f32[2,512]{1,0:T(2,128)} %bitcast.5), custom_call_target="tpu_custom_call" | custom-call | tf_op jit(solution)/shard_map/moe/pallas_call | solution.py:341
  100.9 1.6 %copy.9 = bf16[512,128]{1,0:T(8,128)(2,1)} copy(bf16[512,128]{1,0:T(8,128)(2,1)} %moe.1) | data formatting | bytes 262144

commit v5 on v4

--- a/solution.py
+++ b/solution.py
@@ -11,19 +11,18 @@
 F32 = jnp.float32
 BF16 = jnp.bfloat16
 CHIPS = 4
+PLANE = ((2, 2), (1, 2), (2, 1), (2, 3), (3, 2), (0, 2), (1, 1), (1, 3), (2, 0), (3, 1), (3, 3), (0, 1), (0, 3), (1, 0), (3, 0))
 EPG = 8
 SLOTS = 8
-ORDER = ('D0', 'H3', 'D1', 'S0', 'S1', 'E0', 'E1', 'C0', 'A0', 'C1', 'A1', 'X1', 'X0')
+ORDER = ('D0', 'H3', 'D1', 'S0', 'S1', 'E0', 'E1', 'C0', 'A0', 'C1', 'A1', 'B1', 'B0', 'G1', 'G0')
 RETURNS = {
     'A0': ((0,), 0, 4, True),
     'A1': ((1,), 0, 4, True),
-    'B0': ((0,), 4, 12, True),
-    'B1': ((1,), 4, 12, True),
-    'G0': ((0,), 12, 32, True),
-    'G1': ((1,), 12, 32, True),
+    'B0': ((0,), 4, 10, True),
+    'B1': ((1,), 4, 10, True),
+    'G0': ((0,), 10, 32, True),
+    'G1': ((1,), 10, 32, True),
     'W': ((0, 1), 0, 32, False),
-    'X0': ((0,), 4, 32, True),
-    'X1': ((1,), 4, 32, True),
 }
 NB = 2
 HOPS = (1, 2, 4, 6)
@@ -81,9 +80,9 @@
         pl.semaphore_signal(barrier, inc=1, device_id=peer, device_id_type=MESH)
 
     if tp_count > 1:
-        @pl.loop(1, tp_count)
-        def _(k):
-            pl.semaphore_signal(barrier, inc=1, device_id={"tp": lax.rem(t + k, tp_count)}, device_id_type=MESH)
+        for dy, dx in PLANE:
+            peer = lax.rem(t // CHIPS + dy, CHIPS) * CHIPS + lax.rem(t + dx, CHIPS)
+            pl.semaphore_signal(barrier, inc=1, device_id={"tp": peer}, device_id_type=MESH)
 
     for cp in weight_copies:
         cp.start()
@@ -133,9 +132,8 @@
     pl.semaphore_wait(barrier, 3 + (tp_count - 1))
 
     if tp_count > 1:
-        @pl.loop(1, tp_count)
-        def _(k):
-            peer = lax.rem(t + k, tp_count)
+        for dy, dx in PLANE:
+            peer = lax.rem(t // CHIPS + dy, CHIPS) * CHIPS + lax.rem(t + dx, CHIPS)
             pltpu.make_async_remote_copy(
                 src_ref=tok_v.at[pl.ds(peer * rows, rows)], dst_ref=xin.at[t],
                 send_sem=tp_send, recv_sem=tp_recv, device_id={"tp": peer}, device_id_type=MESH,
@@ -306,9 +304,8 @@
     mine = pltpu.make_async_copy(mx.at[t], out.at[pl.ds(t * rows, rows)], in_sem.at[2])
     mine.start()
     if tp_count > 1:
-        @pl.loop(1, tp_count)
-        def _(k):
-            peer = lax.rem(t + k, tp_count)
+        for dy, dx in PLANE:
+            peer = lax.rem(t // CHIPS + dy, CHIPS) * CHIPS + lax.rem(t + dx, CHIPS)
             pltpu.make_async_remote_copy(
                 src_ref=mx.at[peer], dst_ref=out.at[pl.ds(t * rows, rows)],
                 send_sem=fin_send, recv_sem=fin_recv, device_id={"tp": peer}, device_id_type=MESH,

time: 103 us -> 102 us (level)
  the two profiles are of different devices: /device:TPU:160 before, /device:TPU:128 now
where the time goes in v5:
time: 102 us
  Pallas kernels  100 us (98%)
  local copies, waits for them, and re-layouts  1.57 us (2%)
    pallas_call x1, Pallas kernels, local(): pl.pallas_call(partial(body, ep_count, tp_count), out_shape=jax.ShapeDtyp...  100 us

profile of v5, /device:TPU:128, one launch (start us, length us, event | category | flops | bytes accessed | tf_op | source)
XLA Modules:
  0.0 101.6 jit_solution(14168539705807306972)
XLA Ops:
  0.0 100.0 %moe.1 = bf16[512,128]{1,0:T(8,128)(2,1)} custom-call(bf16[512,128]{1,0:T(8,128)(2,1)} %tokens.1, f32[1,2048]{1,0:T(1,128)} %bitcast.3, bf16[1,2048,512]{2,1,0:T(8,128)(2,1)} %gate_hbm.1, bf16[1,2048,512]{2,1,0:T(8,128)(2,1)} %up_hbm.1, bf16[1,512,2048]{2,1,0:T(8,128)(2,1)} %down_hbm.1, s32[2,512]{1,0:T(2,128)} %bitcast.4, f32[2,512]{1,0:T(2,128)} %bitcast.5), custom_call_target="tpu_custom_call" | custom-call | tf_op jit(solution)/shard_map/moe/pallas_call | solution.py:338
  100.0 1.6 %copy.9 = bf16[512,128]{1,0:T(8,128)(2,1)} copy(bf16[512,128]{1,0:T(8,128)(2,1)} %moe.1) | data formatting | bytes 262144
